TPU v7x, 512 devices: a whole 4x8x8 slice. The times are simulated.
512 devices in a mesh: sp: 32 (over z, x), dp: 16 (over y, core).
Axes of the slice: x: 4, y: 8, z: 8, core: 2. Of those that a mesh axis runs over, the one named last changes fastest.
Arguments:
- query_rows: bfloat16 [16, 4096, 2048], P('dp', 'sp'), may hold values from -6 to 6
- key_rows: bfloat16 [16, 4096, 2048], P('dp', 'sp'), may hold values from -6 to 6
- value_rows: bfloat16 [16, 4096, 2048], P('dp', 'sp'), may hold values from -6 to 6
- decay_low: bfloat16 [16, 4096, 128], P('dp', 'sp'), may hold values from -5 to 5
- rate_low: bfloat16 [16, 4096, 128], P('dp', 'sp'), may hold values from -4 to 4
- decay_up: bfloat16 [128, 2048], replicated, may hold values from -0.5 to 0.5
- rate_up: bfloat16 [128, 2048], replicated, may hold values from -0.5 to 0.5
- decay_base: float32 [2048], replicated, may hold values from -12 to -2
- norm_gain: float32 [2048], replicated, may hold values from 0.1 to 1.9
- out_weight: bfloat16 [2048, 2048], P(None, 'dp'), may hold values from -0.125 to 0.125
Outputs:
- layer_out: bfloat16 [16, 4096, 2048], P('dp', 'sp')
All inputs are finite; a program needn't handle non-finite values.
Results may differ from a plain program's by a relative error of at most 0.005.
Values may be sent and summed in bfloat16 or wider, within the bound.
A program may use at most 128 MiB of HBM per device.

v0:
```python
import math

import jax
import jax.numpy as jnp
from jax import lax
from jax.experimental import pallas as pl
from jax.experimental.pallas import tpu as pltpu
from jax.sharding import PartitionSpec as P

HEAD = 64
L = 128
F32 = jnp.float32
BF16 = jnp.bfloat16
MSG = 80


def split(x):
    high = x.astype(BF16)
    return high, (x - high.astype(F32)).astype(BF16)


def mm(a, b):
    return jnp.dot(a, b, preferred_element_type=F32)


def mm_t(a, b):
    return lax.dot_general(a, b, (((1,), (1,)), ((), ())), preferred_element_type=F32)


def t_mm(a, b):
    return lax.dot_general(a, b, (((0,), (0,)), ((), ())), preferred_element_type=F32)


def cols(*parts):
    return jnp.concatenate(parts, axis=1)


def rows(*parts):
    return jnp.concatenate(parts, axis=0)


def grid_index(n=L):
    return (
        lax.broadcasted_iota(jnp.int32, (n, n), 0),
        lax.broadcasted_iota(jnp.int32, (n, n), 1),
    )


def half_masks(dtype, width=L):
    lane = lax.broadcasted_iota(jnp.int32, (1, width), 1) % L
    return (lane < HEAD).astype(dtype), (lane >= HEAD).astype(dtype)


def prepare(pair, refs, s):
    lanes = pl.ds(pl.multiple_of(pair * L, L), L)
    row, col = grid_index()
    first, second = half_masks(BF16)
    decay_pre = (
        refs["base"][:, lanes] + mm(refs["squashed"][...], refs["decay_up"][:, lanes])
    ).astype(BF16)
    rate_pre = mm(refs["rate_low"][...], refs["rate_up"][:, lanes]).astype(BF16)
    log_decay = -math.exp(-0.5) / (1.0 + jnp.exp(-decay_pre.astype(F32)))
    rate = 1.0 / (1.0 + jnp.exp(-rate_pre.astype(F32)))
    tri = (row >= col).astype(BF16)
    running = mm(cols(tri, tri), rows(*split(log_decay)))
    before = running - log_decay
    centre = running[L // 2 : L // 2 + 1]
    final = running[L - 1 : L]
    key = refs["key"][:, lanes].astype(F32)
    query = refs["query"][:, lanes].astype(F32)
    block = (row // HEAD == col // HEAD).astype(BF16)
    total = mm(cols(*split(key * key)), rows(block, block))
    unit = key * lax.rsqrt(1.0 + total)
    erase = unit * rate
    grown = jnp.exp(running - centre)
    shrunk = jnp.exp(centre - running)
    read_mid = query * grown
    erase_from = unit * jnp.exp(before - centre)
    key_to = key * shrunk
    erase_to = erase * shrunk
    up = jnp.exp(centre)
    down = jnp.exp(final - centre)
    s["read_start"][:, lanes] = read_mid * up
    s["erase_start"][:, lanes] = erase_from * up
    s["key_end"][:, lanes] = key_to * down
    s["erase_end"][:, lanes] = erase_to * down
    s["decay"][:, lanes] = jnp.exp(final)
    from_high, from_low = split(rows(erase_from, read_mid))
    left = cols(from_high, from_low)
    strict = row > col
    within = row >= col
    key_high, key_low = split(key_to)
    erase_high, erase_low = split(erase_to)
    for h, mask in enumerate((first, second)):
        head = 2 * pair + h
        a, b = key_high * mask, key_low * mask
        out = mm_t(left, rows(cols(a, a), cols(b, b)))
        out = out[:, :L] + out[:, L:]
        high, low = split(
            rows(jnp.where(strict, out[:L], 0.0), jnp.where(within, out[L:], 0.0))
        )
        s["on_values"][pair, :, h * L : h * L + L] = high
        s["on_values"][pair, :, (2 + h) * L : (3 + h) * L] = low
        a, b = erase_high * mask, erase_low * mask
        out = mm_t(left, rows(cols(a, a), cols(b, b)))
        out = out[:, :L] + out[:, L:]
        high, low = split(jnp.where(within, out[L:], 0.0))
        s["read_erase"][pair, :, h * L : h * L + L] = high
        s["read_erase"][pair, :, (2 + h) * L : (3 + h) * L] = low
        pairs = jnp.where(strict, out[:L], 0.0)
        high, low = split(pairs)
        s["lower"][head, :, :L] = high
        s["lower"][head, :, L:] = low
        next_to = (row // 2 == col // 2) & (row != col)
        s["inverse"][head] = (row == col).astype(F32) - jnp.where(next_to, pairs, 0.0)


def times(left, right):
    a, b = split(right)
    row = cols(a, b)
    out = mm(left, rows(row, row))
    return out[:, :L] + out[:, L:]


def refine(head0, count, level, s):
    row, col = grid_index()
    mask = ((row >> (level + 1)) == (col >> (level + 1))) & ((row >> level) != (col >> level))
    mask = mask.astype(BF16)
    mask = cols(mask, mask)
    held = [s["inverse"][head0 + i] for i in range(count)]
    below = [times(s["lower"][head0 + i] * mask, held[i]) for i in range(count)]
    for i in range(count):
        s["inverse"][head0 + i] = held[i] - times(cols(*split(held[i])), below[i])


def finish(pair, refs, s, out):
    lanes = pl.ds(pl.multiple_of(pair * L, L), L)
    first, second = half_masks(BF16)
    first2, second2 = half_masks(BF16, 2 * L)
    value = refs["value"][:, lanes]
    both = rows(value * first, value * second)
    seen = mm(s["on_values"][pair], rows(both, both))
    carried, local = seen[:L], seen[L:]

    def on_pair(left, right):
        high, low = split(right)
        high = rows(high * first2, high * second2)
        low = rows(low * first2, low * second2)
        return mm(left, rows(high, high)) + mm(left[:, : 2 * L], low)

    d0, d1 = split(s["inverse"][2 * pair]), split(s["inverse"][2 * pair + 1])
    solved = on_pair(
        cols(d0[0], d1[0], d0[1], d1[1]), cols(s["erase_start"][:, lanes], carried)
    )
    on_erase = on_pair(s["read_erase"][pair], solved)
    out["read_state"][:, lanes] = s["read_start"][:, lanes] - on_erase[:, :L]
    out["local"][:, lanes] = local - on_erase[:, L:]
    weights, taken = solved[:, :L], solved[:, L:]
    kh, kl = split(s["key_end"][:, lanes])
    eh, el = split(s["erase_end"][:, lanes])
    wh, wl = split(weights)
    th, tl = split(-taken)
    added = t_mm(rows(value, value, th, tl, th), rows(kh, kl, eh, eh, el))
    moved = t_mm(rows(wh, wl, wh), rows(eh, eh, el))
    decay = jnp.broadcast_to(s["decay"][:, lanes], (16, L))
    dh = decay.astype(BF16).astype(F32)
    dl = decay - dh
    low_half = lax.broadcasted_iota(jnp.int32, (HEAD, L), 1) < HEAD
    turn = lambda x: pltpu.roll(x, HEAD, 1)
    out["message"][2 * pair, :HEAD] = jnp.where(
        low_half, added[:HEAD], turn(moved[:HEAD])
    ).astype(BF16)
    out["message"][2 * pair, HEAD:] = jnp.where(low_half[:16], dh, turn(dl)).astype(BF16)
    out["message"][2 * pair + 1, :HEAD] = jnp.where(
        low_half, turn(added[HEAD:]), moved[HEAD:]
    ).astype(BF16)
    out["message"][2 * pair + 1, HEAD:] = jnp.where(low_half[:16], turn(dh), dl).astype(BF16)


LOCAL_IN = (
    "query",
    "key",
    "value",
    "decay_low",
    "rate_low",
    "decay_up",
    "rate_up",
    "base",
)
LOCAL_OUT = ("read_state", "local", "message")


def local_scratch(width):
    pairs = width // L
    wide = lambda: pltpu.VMEM((L, width), F32)
    return dict(
        squashed=pltpu.VMEM((L, L), BF16),
        read_start=wide(),
        erase_start=wide(),
        key_end=wide(),
        erase_end=wide(),
        decay=pltpu.VMEM((1, width), F32),
        on_values=pltpu.VMEM((pairs, 2 * L, 4 * L), BF16),
        read_erase=pltpu.VMEM((pairs, L, 4 * L), BF16),
        lower=pltpu.VMEM((2 * pairs, L, 2 * L), BF16),
        inverse=pltpu.VMEM((2 * pairs, L, L), F32),
    )


def local_phases(refs, s, out, width, group=(2, 8, 2)):
    pairs = width // L
    s["squashed"][...] = jnp.tanh(refs["decay_low"][...].astype(F32)).astype(BF16)
    refs = dict(refs, squashed=s["squashed"])

    @pl.loop(0, pairs // group[0])
    def _(i):
        for j in range(group[0]):
            prepare(i * group[0] + j, refs, s)

    for level in range(1, 7):

        @pl.loop(0, 2 * pairs // group[1])
        def _(i):
            refine(i * group[1], group[1], level, s)

    @pl.loop(0, pairs // group[2])
    def _(i):
        for j in range(group[2]):
            finish(i * group[2] + j, refs, s, out)


def local_kernel(*args, width):
    n_in, n_out = len(LOCAL_IN), len(LOCAL_OUT)
    refs = dict(zip(LOCAL_IN, args[:n_in]))
    out = dict(zip(LOCAL_OUT, args[n_in : n_in + n_out]))
    s = dict(zip(local_scratch(width), args[n_in + n_out :]))
    local_phases(refs, s, out, width)


def run_local(*args):
    width = args[0].shape[1]
    heads = width // HEAD
    vmem = pl.BlockSpec(memory_space=pltpu.VMEM)
    return pl.pallas_call(
        lambda *a: local_kernel(*a, width=width),
        out_shape=(
            jax.ShapeDtypeStruct((L, width), F32),
            jax.ShapeDtypeStruct((L, width), F32),
            jax.ShapeDtypeStruct((heads, MSG, L), BF16),
        ),
        in_specs=[vmem] * len(LOCAL_IN),
        out_specs=(vmem,) * 3,
        scratch_shapes=list(local_scratch(width).values()),
        compiler_params=pltpu.CompilerParams(vmem_limit_bytes=60 * 2**20),
        name="local",
    )(*args)


def scan_kernel(message, states, added, moved, decay):
    count = message.shape[0]
    low_half = lax.broadcasted_iota(jnp.int32, (HEAD, L), 1) < HEAD
    turn = lambda x: pltpu.roll(x, HEAD, 1)

    @pl.loop(0, count)
    def _(n):
        both = message[n, :HEAD].astype(F32)
        added[n] = both
        moved[n] = jnp.where(low_half, turn(both), 0.0).astype(BF16)
        parts = message[n, HEAD:].astype(F32)
        decay[n] = (parts + turn(parts))[:8]

    def step(n, state):
        high, low = split(state)
        states[n] = jnp.where(
            low_half[: HEAD // 2], state[: HEAD // 2], turn(state[HEAD // 2 :])
        ).astype(BF16)
        out = mm(rows(high, low)[:, :HEAD], moved[n])
        state = state * decay[n][:1] - (out[:HEAD] + out[HEAD:]) + added[n]
        return state

    lax.fori_loop(0, count, step, jnp.zeros((HEAD, L), F32))


def run_scan(message):
    count = message.shape[0]
    vmem = pl.BlockSpec(memory_space=pltpu.VMEM)
    return pl.pallas_call(
        scan_kernel,
        out_shape=jax.ShapeDtypeStruct((count, HEAD // 2, L), BF16),
        in_specs=[vmem],
        out_specs=vmem,
        scratch_shapes=[
            pltpu.VMEM((count, HEAD, L), F32),
            pltpu.VMEM((count, HEAD, L), BF16),
            pltpu.VMEM((count, 8, L), F32),
        ],
        name="scan",
    )(message)


def read_pair(pair, read_state, local, states, gain, mix):
    lanes = pl.ds(pl.multiple_of(pair * L, L), L)
    low_half = lax.broadcasted_iota(jnp.int32, (HEAD // 2, L), 1) < HEAD
    turn = lambda x: pltpu.roll(x, HEAD, 1)
    a = states[2 * pair].astype(F32)
    b = states[2 * pair + 1].astype(F32)
    state = rows(
        jnp.where(low_half, a, 0.0),
        jnp.where(low_half, turn(a), 0.0),
        jnp.where(low_half, 0.0, turn(b)),
        jnp.where(low_half, 0.0, b),
    ).astype(BF16)
    readout = mm_t(cols(*split(read_state[:, lanes])), cols(state, state)) + local[:, lanes]
    row, col = grid_index()
    block = (row // HEAD == col // HEAD).astype(BF16)
    block = rows(block, block)
    centred = readout - mm(cols(*split(readout)), block) * (1.0 / HEAD)
    variance = mm(cols(*split(centred * centred)), block) * (1.0 / HEAD)
    mix[:, lanes] = (centred * lax.rsqrt(variance + 1.0) * gain[:, lanes]).astype(BF16)


def output_kernel(read_state, local, states, gain, weight, out, mix):
    pairs = read_state.shape[1] // L

    @pl.loop(0, pairs // 4)
    def _(i):
        for j in range(4):
            read_pair(i * 4 + j, read_state, local, states, gain, mix)

    @pl.loop(0, weight.shape[0] // 2)
    def _(i):
        both = cols(weight[2 * i], weight[2 * i + 1])
        out[:, pl.ds(pl.multiple_of(i * 2 * L, 2 * L), 2 * L)] = mm(mix[...], both).astype(BF16)


def run_output(read_state, local, states, gain, weight):
    vmem = pl.BlockSpec(memory_space=pltpu.VMEM)
    return pl.pallas_call(
        output_kernel,
        out_shape=jax.ShapeDtypeStruct((L, weight.shape[0] * weight.shape[2]), BF16),
        in_specs=[vmem] * 5,
        out_specs=vmem,
        scratch_shapes=[pltpu.VMEM(read_state.shape, BF16)],
        compiler_params=pltpu.CompilerParams(vmem_limit_bytes=60 * 2**20),
        name="output",
    )(read_state, local, states, gain, weight)


def per_device(
    query_rows, key_rows, value_rows, decay_low, rate_low, decay_up, rate_up, decay_base, norm_gain, out_weight
):
    weight = lax.all_gather(out_weight, "dp")
    read_state, local, message = run_local(
        query_rows[0], key_rows[0], value_rows[0], decay_low[0], rate_low[0],
        decay_up, rate_up, decay_base[None],
    )
    got = lax.all_to_all(message, "sp", split_axis=0, concat_axis=0, tiled=True)
    states = run_scan(got)
    starts = lax.all_to_all(states, "sp", split_axis=0, concat_axis=0, tiled=True)
    return run_output(read_state, local, starts, norm_gain[None], weight)[None]


def solution(mesh):
    rows_spec = P("dp", "sp", None)
    return jax.shard_map(
        per_device,
        mesh=mesh,
        in_specs=(rows_spec,) * 5 + (P(), P(), P(), P(), P(None, "dp")),
        out_specs=rows_spec,
        check_vma=False,
    )
```

profile of v0, /device:TPU:32, one launch (start us, length us, event | category | flops | bytes accessed | tf_op | source)
XLA Modules:
  0.0 122.2 jit_solution(15216539611866059591)
XLA Ops:
  6.5 0.0 all-gather.3.cloned.1.call-start
  6.5 0.7 all-gather.3.cloned.1.call-update
  7.3 37.4 %local.1 = (f32[128,2048]{1,0:T(8,128)}, f32[128,2048]{1,0:T(8,128)}, bf16[32,80,128]{2,1,0:T(8,128)(2,1)}) custom-call(bf16[128,2048]{1,0:T(8,128)(2,1)} %bitcast.10, bf16[128,2048]{1,0:T(8,128)(2,1)} %bitcast.11, bf16[128,2048]{1,0:T(8,128)(2,1)} %bitcast.12, bf16[128,128]{1,0:T(8,128)(2,1)} %bitcast.13, bf16[128,128]{1,0:T(8,128)(2,1)} %bitcast.14, ...), custom_call_target="tpu_custom_call" | custom-call | tf_op jit(solution)/shard_map/local/pallas_call | solution.py:244
  44.6 33.5 %all_to_all.10.message = bf16[32,80,128]{2,1,0:T(8,128)(2,1)} all-to-all(bf16[32,80,128]{2,1,0:T(8,128)(2,1)} %get-tuple-element.10), channel_id=1, replica_groups=mesh['sp'=32,'dp'=16] {'sp'}, dimensions={0} | all-to-all | bytes 1310720 | tf_op jit(solution)/shard_map/all_to_all | solution.py:357
  78.1 8.4 %scan.1 = bf16[32,32,128]{2,1,0:T(8,128)(2,1)} custom-call(bf16[32,80,128]{2,1,0:T(8,128)(2,1)} %all_to_all.10.message), custom_call_target="tpu_custom_call" | custom-call | tf_op jit(solution)/shard_map/scan/pallas_call | solution.py:287
  86.5 17.3 %all_to_all.11.states = bf16[32,32,128]{2,1,0:T(8,128)(2,1)} all-to-all(bf16[32,32,128]{2,1,0:T(8,128)(2,1)} %scan.1), channel_id=1, replica_groups=mesh['sp'=32,'dp'=16] {'sp'}, dimensions={0} | all-to-all | bytes 524288 | tf_op jit(solution)/shard_map/all_to_all | solution.py:359
  103.9 0.0 all-gather.3.cloned.1.call-done
  103.9 11.5 %output.1 = bf16[128,2048]{1,0:T(8,128)(2,1)} custom-call(f32[128,2048]{1,0:T(8,128)} %get-tuple-element.8.read_state, f32[128,2048]{1,0:T(8,128)} %get-tuple-element.9.local, bf16[32,32,128]{2,1,0:T(8,128)(2,1)} %all_to_all.11.states, f32[1,2048]{1,0:T(1,128)} %bitcast.16, bf16[16,2048,128]{2,1,0:T(8,128)(2,1)} %bitcast.9), custom_call_target="tpu_custom_call" | custom-call | tf_op jit(solution)/shard_map/output/pallas_call | solution.py:338
Async XLA Ops:
  6.5 97.3 %all-gather.3.cloned.1.call-start = ((), (), s32[]{:S(2)}) async-start(), calls=%async_computation.2 | async-start | bytes 8912896 | tf_op jit(solution)/shard_map/all_gather | solution.py:352
Sparse Core Ops, SparseCore 0:
  9.4 60.1 all-gather.2
where the time goes:
time: 122 us
  Pallas kernels  57.2 us (47%)
  blocking collectives  50.8 us (42%)
  between operations  13.4 us (11%)
    pallas_call x1, Pallas kernels, run_local(): pl.pallas_call(lambda *a: local_kernel(*a, width=width), out_shape=(jax.S...  37.4 us
    all_to_all x1, blocking collectives, per_device(): got = lax.all_to_all(message, 'sp', split_axis=0, concat_axis=0, tiled=True)  33.5 us
    all_to_all x1, blocking collectives, per_device(): lax.all_to_all(states, 'sp', split_axis=0, concat_axis=0, tiled=True)  17.3 us
    pallas_call x1, Pallas kernels, run_output(): pl.pallas_call(output_kernel, out_shape=jax.ShapeDtypeStruct((L, weight.s...  11.5 us
    pallas_call x1, Pallas kernels, run_scan(): pl.pallas_call(scan_kernel, out_shape=jax.ShapeDtypeStruct((count, HEAD /...  8.44 us
  transfers between devices with their start and end apart: 1, of which 0 were waited for; matrix products, arithmetic and copies ran while one was open for 0% of the time, Pallas kernels for 37%

commit v1 on v0

--- a/solution.py
+++ b/solution.py
@@ -1,3 +1,4 @@
+import functools
 import math
 
 import jax
@@ -177,19 +178,6 @@
     out["message"][2 * pair + 1, HEAD:] = jnp.where(low_half[:16], turn(dh), dl).astype(BF16)
 
 
-LOCAL_IN = (
-    "query",
-    "key",
-    "value",
-    "decay_low",
-    "rate_low",
-    "decay_up",
-    "rate_up",
-    "base",
-)
-LOCAL_OUT = ("read_state", "local", "message")
-
-
 def local_scratch(width):
     pairs = width // L
     wide = lambda: pltpu.VMEM((L, width), F32)
@@ -205,97 +193,6 @@
         lower=pltpu.VMEM((2 * pairs, L, 2 * L), BF16),
         inverse=pltpu.VMEM((2 * pairs, L, L), F32),
     )
-
-
-def local_phases(refs, s, out, width, group=(2, 8, 2)):
-    pairs = width // L
-    s["squashed"][...] = jnp.tanh(refs["decay_low"][...].astype(F32)).astype(BF16)
-    refs = dict(refs, squashed=s["squashed"])
-
-    @pl.loop(0, pairs // group[0])
-    def _(i):
-        for j in range(group[0]):
-            prepare(i * group[0] + j, refs, s)
-
-    for level in range(1, 7):
-
-        @pl.loop(0, 2 * pairs // group[1])
-        def _(i):
-            refine(i * group[1], group[1], level, s)
-
-    @pl.loop(0, pairs // group[2])
-    def _(i):
-        for j in range(group[2]):
-            finish(i * group[2] + j, refs, s, out)
-
-
-def local_kernel(*args, width):
-    n_in, n_out = len(LOCAL_IN), len(LOCAL_OUT)
-    refs = dict(zip(LOCAL_IN, args[:n_in]))
-    out = dict(zip(LOCAL_OUT, args[n_in : n_in + n_out]))
-    s = dict(zip(local_scratch(width), args[n_in + n_out :]))
-    local_phases(refs, s, out, width)
-
-
-def run_local(*args):
-    width = args[0].shape[1]
-    heads = width // HEAD
-    vmem = pl.BlockSpec(memory_space=pltpu.VMEM)
-    return pl.pallas_call(
-        lambda *a: local_kernel(*a, width=width),
-        out_shape=(
-            jax.ShapeDtypeStruct((L, width), F32),
-            jax.ShapeDtypeStruct((L, width), F32),
-            jax.ShapeDtypeStruct((heads, MSG, L), BF16),
-        ),
-        in_specs=[vmem] * len(LOCAL_IN),
-        out_specs=(vmem,) * 3,
-        scratch_shapes=list(local_scratch(width).values()),
-        compiler_params=pltpu.CompilerParams(vmem_limit_bytes=60 * 2**20),
-        name="local",
-    )(*args)
-
-
-def scan_kernel(message, states, added, moved, decay):
-    count = message.shape[0]
-    low_half = lax.broadcasted_iota(jnp.int32, (HEAD, L), 1) < HEAD
-    turn = lambda x: pltpu.roll(x, HEAD, 1)
-
-    @pl.loop(0, count)
-    def _(n):
-        both = message[n, :HEAD].astype(F32)
-        added[n] = both
-        moved[n] = jnp.where(low_half, turn(both), 0.0).astype(BF16)
-        parts = message[n, HEAD:].astype(F32)
-        decay[n] = (parts + turn(parts))[:8]
-
-    def step(n, state):
-        high, low = split(state)
-        states[n] = jnp.where(
-            low_half[: HEAD // 2], state[: HEAD // 2], turn(state[HEAD // 2 :])
-        ).astype(BF16)
-        out = mm(rows(high, low)[:, :HEAD], moved[n])
-        state = state * decay[n][:1] - (out[:HEAD] + out[HEAD:]) + added[n]
-        return state
-
-    lax.fori_loop(0, count, step, jnp.zeros((HEAD, L), F32))
-
-
-def run_scan(message):
-    count = message.shape[0]
-    vmem = pl.BlockSpec(memory_space=pltpu.VMEM)
-    return pl.pallas_call(
-        scan_kernel,
-        out_shape=jax.ShapeDtypeStruct((count, HEAD // 2, L), BF16),
-        in_specs=[vmem],
-        out_specs=vmem,
-        scratch_shapes=[
-            pltpu.VMEM((count, HEAD, L), F32),
-            pltpu.VMEM((count, HEAD, L), BF16),
-            pltpu.VMEM((count, 8, L), F32),
-        ],
-        name="scan",
-    )(message)
 
 
 def read_pair(pair, read_state, local, states, gain, mix):
@@ -319,48 +216,337 @@
     mix[:, lanes] = (centred * lax.rsqrt(variance + 1.0) * gain[:, lanes]).astype(BF16)
 
 
-def output_kernel(read_state, local, states, gain, weight, out, mix):
-    pairs = read_state.shape[1] // L
-
-    @pl.loop(0, pairs // 4)
+def scratch(width, n_sp, n_dp):
+    made = local_scratch(width)
+    heads = width // HEAD
+    steps = n_dp // 4
+    dma = pltpu.SemaphoreType.DMA
+    made.update(
+        read_state=pltpu.VMEM((L, width), F32),
+        local=pltpu.VMEM((L, width), F32),
+        message=pltpu.VMEM((heads, MSG, L), BF16),
+        got=pltpu.VMEM((n_sp, MSG, L), BF16),
+        added=pltpu.VMEM((n_sp, HEAD, L), F32),
+        moved=pltpu.VMEM((n_sp, HEAD, L), BF16),
+        kept=pltpu.VMEM((n_sp, 8, L), F32),
+        states=pltpu.VMEM((n_sp, HEAD // 2, L), BF16),
+        starts=pltpu.VMEM((heads, HEAD // 2, L), BF16),
+        mix=pltpu.VMEM((L, width), BF16),
+        weights=pltpu.VMEM((n_dp, width, L), BF16),
+        message_send=dma((n_sp,)),
+        message_recv=dma((n_sp,)),
+        state_send=dma((n_sp,)),
+        state_recv=dma((n_sp,)),
+        ring_send=dma((2 * steps,)),
+        ring_recv=dma((2 * steps,)),
+        twin_send=dma((2 * steps + 1,)),
+        twin_recv=dma((2 * steps + 1,)),
+    )
+    return made
+
+
+INPUTS = (
+    "query",
+    "key",
+    "value",
+    "decay_low",
+    "rate_low",
+    "decay_up",
+    "rate_up",
+    "base",
+    "gain",
+    "weight",
+)
+MESH = pl.DeviceIdType.MESH
+
+
+def remote(src, dst, send, recv, **where):
+    return pltpu.make_async_remote_copy(
+        src_ref=src, dst_ref=dst, send_sem=send, recv_sem=recv, device_id=where, device_id_type=MESH
+    )
+
+
+def whole_kernel(*args, n_sp, n_dp, width, group=(2, 8, 2)):
+    refs = dict(zip(INPUTS, args))
+    out = args[len(INPUTS)]
+    s = dict(zip(scratch(width, n_sp, n_dp), args[len(INPUTS) + 1 :]))
+    pairs = width // L
+    me = lax.axis_index("sp")
+    me_dp = lax.axis_index("dp")
+    core, y, ring = me_dp % 2, me_dp // 2, n_dp // 2
+    steps = ring // 2
+    twin = y * 2 + 1 - core
+    at = lambda offset: ((y + offset + ring) % ring) * 2 + core
+
+    barrier = pltpu.get_barrier_semaphore()
+
+    @pl.loop(1, n_sp)
+    def _(j):
+        pl.semaphore_signal(
+            barrier, inc=1, device_id={"sp": (me + j) % n_sp}, device_id_type=MESH
+        )
+
+    for peer in (twin, at(1), at(-1)):
+        pl.semaphore_signal(barrier, inc=1, device_id={"dp": peer}, device_id_type=MESH)
+    pl.semaphore_wait(barrier, n_sp + 2)
+
+    def part(ref, way, step):
+        if step < steps - 1:
+            return ref
+        half = width // 2
+        return ref.at[pl.ds(way * half, half)]
+
+    def ring_copy(way, step):
+        block = at(-step if way == 0 else step)
+        src = refs["weight"] if step == 0 else s["weights"].at[block]
+        return remote(
+            part(src, way, step),
+            part(s["weights"].at[block], way, step),
+            s["ring_send"].at[way * steps + step],
+            s["ring_recv"].at[way * steps + step],
+            dp=at(1 if way == 0 else -1),
+        )
+
+    def ring_arrival(way, step):
+        block = at(-1 - step if way == 0 else 1 + step)
+        here = part(s["weights"].at[block], way, step)
+        return remote(
+            here,
+            here,
+            s["ring_send"].at[way * steps + step],
+            s["ring_recv"].at[way * steps + step],
+            dp=at(1 if way == 0 else -1),
+        )
+
+    def twin_copy(way, step):
+        index = way * steps + step
+        here = part(s["weights"].at[at(-1 - step if way == 0 else 1 + step)], way, step)
+        return remote(here, here, s["twin_send"].at[index], s["twin_recv"].at[index], dp=twin)
+
+    def twin_arrival(way, step):
+        index = way * steps + step
+        offset = -1 - step if way == 0 else 1 + step
+        block = ((y + offset + ring) % ring) * 2 + 1 - core
+        here = part(s["weights"].at[block], way, step)
+        return remote(here, here, s["twin_send"].at[index], s["twin_recv"].at[index], dp=twin)
+
+    twin_own = remote(
+        refs["weight"],
+        s["weights"].at[me_dp],
+        s["twin_send"].at[2 * steps],
+        s["twin_recv"].at[2 * steps],
+        dp=twin,
+    )
+    twin_first = remote(
+        refs["weight"],
+        s["weights"].at[twin],
+        s["twin_send"].at[2 * steps],
+        s["twin_recv"].at[2 * steps],
+        dp=twin,
+    )
+
+    def forward(step):
+        for way in range(2):
+            ring_arrival(way, step).wait_recv()
+            if step + 1 < steps:
+                ring_copy(way, step + 1).start()
+            twin_copy(way, step).start()
+
+    for way in range(2):
+        ring_copy(way, 0).start()
+    twin_own.start()
+    s["weights"][me_dp] = refs["weight"][...]
+
+    s["squashed"][...] = jnp.tanh(refs["decay_low"][...].astype(F32)).astype(BF16)
+    refs["squashed"] = s["squashed"]
+    turned = lambda p: (p + me // 2) % pairs
+
+    @pl.loop(0, pairs // group[0])
     def _(i):
-        for j in range(4):
-            read_pair(i * 4 + j, read_state, local, states, gain, mix)
-
-    @pl.loop(0, weight.shape[0] // 2)
+        for j in range(group[0]):
+            prepare(turned(i * group[0] + j), refs, s)
+
+    forward(0)
+    for level in range(1, 7):
+
+        @pl.loop(0, 2 * pairs // group[1])
+        def _(i):
+            refine(i * group[1], group[1], level, s)
+
+        if level == 3 and steps > 2:
+            forward(1)
+
+    def message_copy(head):
+        return remote(
+            s["message"].at[head],
+            s["got"].at[me],
+            s["message_send"].at[head],
+            s["message_recv"].at[me],
+            sp=head,
+        )
+
+    def send_messages(i):
+        for j in range(group[2]):
+            for h in range(2):
+                head = 2 * turned(i * group[2] + j) + h
+
+                @pl.when(head != me)
+                def _():
+                    message_copy(head).start()
+
+    @pl.loop(0, pairs // group[2])
     def _(i):
-        both = cols(weight[2 * i], weight[2 * i + 1])
-        out[:, pl.ds(pl.multiple_of(i * 2 * L, 2 * L), 2 * L)] = mm(mix[...], both).astype(BF16)
-
-
-def run_output(read_state, local, states, gain, weight):
-    vmem = pl.BlockSpec(memory_space=pltpu.VMEM)
-    return pl.pallas_call(
-        output_kernel,
-        out_shape=jax.ShapeDtypeStruct((L, weight.shape[0] * weight.shape[2]), BF16),
-        in_specs=[vmem] * 5,
-        out_specs=vmem,
-        scratch_shapes=[pltpu.VMEM(read_state.shape, BF16)],
-        compiler_params=pltpu.CompilerParams(vmem_limit_bytes=60 * 2**20),
-        name="output",
-    )(read_state, local, states, gain, weight)
-
-
-def per_device(
-    query_rows, key_rows, value_rows, decay_low, rate_low, decay_up, rate_up, decay_base, norm_gain, out_weight
-):
-    weight = lax.all_gather(out_weight, "dp")
-    read_state, local, message = run_local(
-        query_rows[0], key_rows[0], value_rows[0], decay_low[0], rate_low[0],
-        decay_up, rate_up, decay_base[None],
-    )
-    got = lax.all_to_all(message, "sp", split_axis=0, concat_axis=0, tiled=True)
-    states = run_scan(got)
-    starts = lax.all_to_all(states, "sp", split_axis=0, concat_axis=0, tiled=True)
-    return run_output(read_state, local, starts, norm_gain[None], weight)[None]
+        for j in range(group[2]):
+            finish(turned(i * group[2] + j), refs, s, s)
+
+        @pl.when(i > 0)
+        def _():
+            send_messages(i - 1)
+
+    s["got"][me] = s["message"][me]
+    send_messages(pairs // group[2] - 1)
+    if steps > 3:
+        forward(2)
+
+    low_half = lax.broadcasted_iota(jnp.int32, (HEAD, L), 1) < HEAD
+    turn = lambda x: pltpu.roll(x, HEAD, 1)
+
+    def unpack(n):
+        both = s["got"][n, :HEAD].astype(F32)
+        s["added"][n] = both
+        s["moved"][n] = jnp.where(low_half, turn(both), 0.0).astype(BF16)
+        parts = s["got"][n, HEAD:].astype(F32)
+        s["kept"][n] = (parts + turn(parts))[:8]
+
+    unpack(me)
+
+    @pl.loop(1, n_sp)
+    def _(j):
+        n = (me + j) % n_sp
+        remote(
+            s["got"].at[n],
+            s["got"].at[n],
+            s["message_send"].at[n],
+            s["message_recv"].at[n],
+            sp=n,
+        ).wait_recv()
+        unpack(n)
+
+    def state_copy(n):
+        return remote(
+            s["states"].at[n],
+            s["starts"].at[me],
+            s["state_send"].at[n],
+            s["state_recv"].at[me],
+            sp=n,
+        )
+
+    def step(n, state):
+        high, low = split(state)
+        s["states"][n] = jnp.where(
+            low_half[: HEAD // 2], state[: HEAD // 2], turn(state[HEAD // 2 :])
+        ).astype(BF16)
+        moved = mm(rows(high, low)[:, :HEAD], s["moved"][n])
+
+        @pl.when((n > 0) & (n - 1 != me))
+        def _():
+            state_copy(n - 1).start()
+
+        return state * s["kept"][n][:1] - (moved[:HEAD] + moved[HEAD:]) + s["added"][n]
+
+    lax.fori_loop(0, n_sp, step, jnp.zeros((HEAD, L), F32))
+    s["starts"][me] = s["states"][me]
+
+    @pl.when(me != n_sp - 1)
+    def _():
+        state_copy(n_sp - 1).start()
+
+    forward(steps - 1)
+
+    @pl.loop(1, n_sp)
+    def _(j):
+        n = (me + j) % n_sp
+        remote(
+            s["starts"].at[n],
+            s["starts"].at[n],
+            s["state_send"].at[n],
+            s["state_recv"].at[n],
+            sp=n,
+        ).wait_recv()
+
+    @pl.loop(0, pairs // group[2])
+    def _(i):
+        for j in range(group[2]):
+            read_pair(
+                i * group[2] + j, s["read_state"], s["local"], s["starts"], refs["gain"], s["mix"]
+            )
+
+    twin_first.wait_recv()
+    for way in range(2):
+        for k in range(steps):
+            twin_arrival(way, k).wait_recv()
+
+    @pl.loop(0, n_dp // 2)
+    def _(i):
+        both = cols(s["weights"][2 * i], s["weights"][2 * i + 1])
+        out[:, pl.ds(pl.multiple_of(i * 2 * L, 2 * L), 2 * L)] = mm(s["mix"][...], both).astype(
+            BF16
+        )
+
+    twin_own.wait_send()
+    for way in range(2):
+        for k in range(steps):
+            ring_copy(way, k).wait_send()
+            twin_copy(way, k).wait_send()
+
+    @pl.loop(1, n_sp)
+    def _(j):
+        n = (me + j) % n_sp
+        message_copy(n).wait_send()
+        state_copy(n).wait_send()
 
 
 def solution(mesh):
+    n_sp, n_dp = mesh.shape["sp"], mesh.shape["dp"]
+
+    def per_device(
+        query_rows,
+        key_rows,
+        value_rows,
+        decay_low,
+        rate_low,
+        decay_up,
+        rate_up,
+        decay_base,
+        norm_gain,
+        out_weight,
+    ):
+        width = query_rows.shape[2]
+        vmem = pl.BlockSpec(memory_space=pltpu.VMEM)
+        out = pl.pallas_call(
+            functools.partial(whole_kernel, n_sp=n_sp, n_dp=n_dp, width=width),
+            out_shape=jax.ShapeDtypeStruct((L, n_dp * L), BF16),
+            in_specs=[vmem] * len(INPUTS),
+            out_specs=vmem,
+            scratch_shapes=list(scratch(width, n_sp, n_dp).values()),
+            compiler_params=pltpu.CompilerParams(
+                collective_id=0, has_side_effects=True, vmem_limit_bytes=60 * 2**20
+            ),
+            name="mixer",
+        )(
+            query_rows[0],
+            key_rows[0],
+            value_rows[0],
+            decay_low[0],
+            rate_low[0],
+            decay_up,
+            rate_up,
+            decay_base[None],
+            norm_gain[None],
+            out_weight,
+        )
+        return out[None]
+
     rows_spec = P("dp", "sp", None)
     return jax.shard_map(
         per_device,

time: 122 us -> 93.9 us (0.77)
  the two profiles are of different devices: /device:TPU:32 before, /device:TPU:1 now
where the time goes in v1:
time: 93.9 us; the launch traced here: 93.2 us
  Pallas kernels  91.3 us (97%)
  local copies, waits for them, and re-layouts  1.88 us (2%)
    pallas_call x1, Pallas kernels, per_device(): pl.pallas_call(functools.partial(whole_kernel, n_sp=n_sp, n_dp=n_dp, widt...  91.3 us
    unnamed x1, local copies, waits for them, and re-layouts  1.88 us

profile of v1, /device:TPU:1, one launch (start us, length us, event | category | flops | bytes accessed | tf_op | source)
XLA Modules:
  0.0 93.2 jit_solution(2929120560595170007)
XLA Ops:
  0.0 91.3 %mixer.1 = bf16[128,2048]{1,0:T(8,128)(2,1)} custom-call(bf16[128,2048]{1,0:T(8,128)(2,1)} %bitcast.9, bf16[128,2048]{1,0:T(8,128)(2,1)} %bitcast.10, bf16[128,2048]{1,0:T(8,128)(2,1)} %bitcast.11, bf16[128,128]{1,0:T(8,128)(2,1)} %bitcast.12, bf16[128,128]{1,0:T(8,128)(2,1)} %bitcast.13, bf16[128,2048]{1,0:T(8,128)(2,1)} %args_5_.4, ...), custom_call_target="tpu_custom_call" | custom-call | tf_op jit(solution)/shard_map/mixer/pallas_call | solution.py:526
  91.3 1.9 %copy.12 = bf16[1,128,2048]{2,1,0:T(8,128)(2,1)} copy(bf16[1,128,2048]{2,1,0:T(8,128)(2,1)} %bitcast.8) | data formatting | bytes 1048576

commit v2 on v1

v2 whole, which is shorter than its diff:
```python
import functools
import math

import jax
import jax.numpy as jnp
from jax import lax
from jax.experimental import pallas as pl
from jax.experimental.pallas import tpu as pltpu
from jax.sharding import PartitionSpec as P

HEAD = 64
L = 128
F32 = jnp.float32
BF16 = jnp.bfloat16
TAIL = 8
MSG = HEAD + TAIL
QUARTERS = 4
SPAN = 4


def split(x):
    high = x.astype(BF16)
    return high, (x - high.astype(F32)).astype(BF16)


def mm(a, b):
    return jnp.dot(a, b, preferred_element_type=F32)


def mm_t(a, b):
    return lax.dot_general(a, b, (((1,), (1,)), ((), ())), preferred_element_type=F32)


def t_mm(a, b):
    return lax.dot_general(a, b, (((0,), (0,)), ((), ())), preferred_element_type=F32)


def cols(*parts):
    return jnp.concatenate(parts, axis=1)


def rows(*parts):
    return jnp.concatenate(parts, axis=0)


def grid_index(n=L):
    return (
        lax.broadcasted_iota(jnp.int32, (n, n), 0),
        lax.broadcasted_iota(jnp.int32, (n, n), 1),
    )


def half_masks(dtype, width=L):
    lane = lax.broadcasted_iota(jnp.int32, (1, width), 1) % L
    return (lane < HEAD).astype(dtype), (lane >= HEAD).astype(dtype)


def prepare_group(chosen, refs, s):
    row, col = grid_index()
    first, second = half_masks(BF16)
    tri = (row >= col).astype(BF16)
    tri = cols(tri, tri)
    block = (row // HEAD == col // HEAD).astype(BF16)
    block = rows(block, block)
    held = []
    for pair in chosen:
        lanes = pl.ds(pl.multiple_of(pair * L, L), L)
        decay_pre = (
            refs["base"][:, lanes] + mm(s["squashed"][...], refs["decay_up"][:, lanes])
        ).astype(BF16)
        rate_pre = mm(refs["rate_low"][...], refs["rate_up"][:, lanes]).astype(BF16)
        log_decay = -math.exp(-0.5) / (1.0 + jnp.exp(-decay_pre.astype(F32)))
        rate = 1.0 / (1.0 + jnp.exp(-rate_pre.astype(F32)))
        running = mm(tri, rows(*split(log_decay)))
        key = refs["key"][:, lanes].astype(F32)
        total = mm(cols(*split(key * key)), block)
        held.append((pair, lanes, log_decay, rate, running, key, total))
    lefts = []
    for pair, lanes, log_decay, rate, running, key, total in held:
        before = running - log_decay
        centre = running[L // 2 : L // 2 + 1]
        final = running[L - 1 : L]
        query = refs["query"][:, lanes].astype(F32)
        unit = key * lax.rsqrt(1.0 + total)
        shrunk = jnp.exp(centre - running)
        read_mid = query * jnp.exp(running - centre)
        erase_from = unit * jnp.exp(before - centre)
        key_to = key * shrunk
        erase_to = unit * rate * shrunk
        up = jnp.exp(centre)
        down = jnp.exp(final - centre)
        s["read_start"][:, lanes] = read_mid * up
        s["erase_start"][:, lanes] = erase_from * up
        s["key_end"][:, lanes] = key_to * down
        s["erase_end"][:, lanes] = erase_to * down
        s["decay"][:, lanes] = jnp.exp(final)
        left = cols(*split(rows(erase_from, read_mid)))
        high, low = split(rows(key_to, erase_to))
        lefts.append((pair, left, high, low))
    for pair, left, high, low in lefts:
        for h, mask in enumerate((first, second)):
            a, b = high * mask, low * mask
            out = mm_t(left, cols(a, a)) + mm_t(left, cols(b, b))
            strict, within = s["strict"][...], s["within"][...]
            high_on, low_on = split(out[:L, :L] * strict)
            s["key_pairs"][pair, :, h * L : h * L + L] = high_on
            s["key_pairs"][pair, :, (2 + h) * L : (3 + h) * L] = low_on
            high_on, low_on = split(out[L:, :L] * within)
            s["read_keys"][pair, :, h * L : h * L + L] = high_on
            s["read_keys"][pair, :, (2 + h) * L : (3 + h) * L] = low_on
            high_on, low_on = split(out[L:, L:] * within)
            s["read_erase"][pair, :, h * L : h * L + L] = high_on
            s["read_erase"][pair, :, (2 + h) * L : (3 + h) * L] = low_on
            pairs = out[:L, L:] * strict
            high_on, low_on = split(pairs)
            head = 2 * pair + h
            s["lower"][head, :, :L] = high_on
            s["lower"][head, :, L:] = low_on
            s["inverse"][head] = s["eye"][...] - pairs * s["next_to"][...]


def times(left, right):
    a, b = split(right)
    row = cols(a, b)
    out = mm(left, rows(row, row))
    return out[:, :L] + out[:, L:]


def refine_group(chosen, level, s):
    held = [s["inverse"][head] for head in chosen]
    below = [
        times(s["lower"][head] * s["levels"][level], held[i]) for i, head in enumerate(chosen)
    ]
    for i, head in enumerate(chosen):
        s["inverse"][head] = held[i] - times(cols(*split(held[i])), below[i])


def fill_masks(s):
    row, col = grid_index()
    s["strict"][...] = (row > col).astype(F32)
    s["within"][...] = (row >= col).astype(F32)
    s["eye"][...] = (row == col).astype(F32)
    s["next_to"][...] = ((row // 2 == col // 2) & (row != col)).astype(F32)
    for level in range(1, 7):
        mask = (row >> (level + 1)) == (col >> (level + 1))
        mask = (mask & ((row >> level) != (col >> level))).astype(BF16)
        s["levels"][level - 1] = cols(mask, mask)


def on_pair(left, high, low):
    first, second = half_masks(BF16, 2 * L)
    high = rows(high * first, high * second)
    low = rows(low * first, low * second)
    return mm(left, rows(high, high)) + mm(left[:, : 2 * L], low)


def doubled(value):
    first, second = half_masks(BF16)
    both = rows(value * first, value * second)
    return rows(both, both)


def solve_group(chosen, refs, s):
    lanes_of = [pl.ds(pl.multiple_of(pair * L, L), L) for pair in chosen]
    carried = [
        mm(s["key_pairs"][pair], doubled(refs["value"][:, lanes]))
        for pair, lanes in zip(chosen, lanes_of)
    ]
    solved = []
    for pair, lanes, carry in zip(chosen, lanes_of, carried):
        d0, d1 = split(s["inverse"][2 * pair]), split(s["inverse"][2 * pair + 1])
        high, low = split(cols(s["erase_start"][:, lanes], carry))
        solved.append(split(on_pair(cols(d0[0], d1[0], d0[1], d1[1]), high, low)))
    low_half = lax.broadcasted_iota(jnp.int32, (HEAD, L), 1) < HEAD
    turn = lambda x: pltpu.roll(x, HEAD, 1)
    for pair, lanes, (high, low) in zip(chosen, lanes_of, solved):
        s["solved"][pair, :, : 2 * L] = high
        s["solved"][pair, :, 2 * L :] = low
        ends = cols(*split(s["erase_end"][:, lanes]))
        moved = t_mm(rows(high, low), rows(ends, ends))
        moved = moved[:, :L] + moved[:, L:]
        added = t_mm(refs["value"][:, lanes], cols(*split(s["key_end"][:, lanes])))
        added = added[:, :L] + added[:, L:] - moved[L:]
        moved = moved[:L]
        decay = jnp.broadcast_to(s["decay"][:, lanes], (TAIL, L))
        dh = decay.astype(BF16).astype(F32)
        dl = decay - dh
        s["message"][2 * pair, :HEAD] = jnp.where(
            low_half, added[:HEAD], turn(moved[:HEAD])
        ).astype(BF16)
        s["message"][2 * pair, HEAD:] = jnp.where(low_half[:TAIL], dh, turn(dl)).astype(BF16)
        s["message"][2 * pair + 1, :HEAD] = jnp.where(
            low_half, turn(added[HEAD:]), moved[HEAD:]
        ).astype(BF16)
        s["message"][2 * pair + 1, HEAD:] = jnp.where(low_half[:TAIL], turn(dh), dl).astype(BF16)


def local_group(chosen, refs, s):
    for pair in chosen:
        lanes = pl.ds(pl.multiple_of(pair * L, L), L)
        both = s["solved"][pair]
        on_erase = on_pair(s["read_erase"][pair], both[:, : 2 * L], both[:, 2 * L :])
        local = mm(s["read_keys"][pair], doubled(refs["value"][:, lanes]))
        s["read_state"][:, lanes] = s["read_start"][:, lanes] - on_erase[:, :L]
        s["local"][:, lanes] = local - on_erase[:, L:]


def read_group(chosen, refs, s):
    low_half = lax.broadcasted_iota(jnp.int32, (HEAD // 2, L), 1) < HEAD
    turn = lambda x: pltpu.roll(x, HEAD, 1)
    row, col = grid_index()
    block = (row // HEAD == col // HEAD).astype(BF16)
    block = rows(block, block)
    lanes_of = [pl.ds(pl.multiple_of(pair * L, L), L) for pair in chosen]
    readouts = []
    for pair, lanes in zip(chosen, lanes_of):
        a = s["starts"][2 * pair].astype(F32)
        b = s["starts"][2 * pair + 1].astype(F32)
        state = rows(
            jnp.where(low_half, a, 0.0),
            jnp.where(low_half, turn(a), 0.0),
            jnp.where(low_half, 0.0, turn(b)),
            jnp.where(low_half, 0.0, b),
        ).astype(BF16)
        readouts.append(
            mm_t(cols(*split(s["read_state"][:, lanes])), cols(state, state)) + s["local"][:, lanes]
        )
    centres = [x - mm(cols(*split(x)), block) * (1.0 / HEAD) for x in readouts]
    spreads = [mm(cols(*split(x * x)), block) * (1.0 / HEAD) for x in centres]
    for lanes, centred, variance in zip(lanes_of, centres, spreads):
        s["mix"][:, lanes] = (centred * lax.rsqrt(variance + 1.0) * refs["gain"][:, lanes]).astype(
            BF16
        )


def local_scratch(width):
    pairs = width // L
    wide = lambda: pltpu.VMEM((L, width), F32)
    return dict(
        squashed=pltpu.VMEM((L, L), BF16),
        read_start=wide(),
        erase_start=wide(),
        key_end=wide(),
        erase_end=wide(),
        decay=pltpu.VMEM((1, width), F32),
        key_pairs=pltpu.VMEM((pairs, L, 4 * L), BF16),
        read_keys=pltpu.VMEM((pairs, L, 4 * L), BF16),
        solved=pltpu.VMEM((pairs, L, 4 * L), BF16),
        strict=pltpu.VMEM((L, L), F32),
        within=pltpu.VMEM((L, L), F32),
        eye=pltpu.VMEM((L, L), F32),
        next_to=pltpu.VMEM((L, L), F32),
        levels=pltpu.VMEM((6, L, 2 * L), BF16),
        read_erase=pltpu.VMEM((pairs, L, 4 * L), BF16),
        lower=pltpu.VMEM((2 * pairs, L, 2 * L), BF16),
        inverse=pltpu.VMEM((2 * pairs, L, L), F32),
    )


def scratch(width, n_sp, n_dp):
    made = local_scratch(width)
    heads = width // HEAD
    chunks = n_dp // 4 * QUARTERS
    dma = pltpu.SemaphoreType.DMA
    made.update(
        read_state=pltpu.VMEM((L, width), F32),
        local=pltpu.VMEM((L, width), F32),
        message=pltpu.VMEM((heads, MSG, L), BF16),
        got=pltpu.VMEM((n_sp, MSG, L), BF16),
        added=pltpu.VMEM((n_sp, HEAD, L), F32),
        moved=pltpu.VMEM((n_sp, HEAD, L), BF16),
        kept=pltpu.VMEM((n_sp, 8, L), F32),
        prefix=pltpu.VMEM((n_sp, 2 * HEAD, L), F32),
        entry=pltpu.VMEM((n_sp // SPAN, HEAD, L), F32),
        states=pltpu.VMEM((n_sp, HEAD // 2, L), BF16),
        starts=pltpu.VMEM((heads, HEAD // 2, L), BF16),
        mix=pltpu.VMEM((L, width), BF16),
        weights=pltpu.VMEM((n_dp, width, L), BF16),
        message_send=dma((n_sp,)),
        message_recv=dma((n_sp,)),
        state_send=dma((n_sp,)),
        state_recv=dma((n_sp,)),
        ring_send=dma((2 * chunks,)),
        ring_recv=dma((2 * chunks,)),
        twin_send=dma((2 * chunks + 1,)),
        twin_recv=dma((2 * chunks + 1,)),
    )
    return made


INPUTS = (
    "query",
    "key",
    "value",
    "decay_low",
    "rate_low",
    "decay_up",
    "rate_up",
    "base",
    "gain",
    "weight",
)
MESH = pl.DeviceIdType.MESH


def remote(src, dst, send, recv, **where):
    return pltpu.make_async_remote_copy(
        src_ref=src, dst_ref=dst, send_sem=send, recv_sem=recv, device_id=where, device_id_type=MESH
    )


def whole_kernel(*args, n_sp, n_dp, width, schedule):
    refs = dict(zip(INPUTS, args))
    out = args[len(INPUTS)]
    s = dict(zip(scratch(width, n_sp, n_dp), args[len(INPUTS) + 1 :]))
    pairs = width // L
    half = pairs // 2
    me = lax.axis_index("sp")
    me_dp = lax.axis_index("dp")
    core, y, ring = me_dp % 2, me_dp // 2, n_dp // 2
    steps = ring // 2
    twin = y * 2 + 1 - core
    at = lambda offset, c: ((y + offset + ring) % ring) * 2 + c
    barrier = pltpu.get_barrier_semaphore()

    def greet():
        @pl.loop(1, n_sp)
        def _(j):
            pl.semaphore_signal(
                barrier, inc=1, device_id={"sp": (me + j) % n_sp}, device_id_type=MESH
            )

        for peer in (twin, at(1, core), at(-1, core)):
            pl.semaphore_signal(barrier, inc=1, device_id={"dp": peer}, device_id_type=MESH)

    def met():
        pl.semaphore_wait(barrier, n_sp + 2)

    order = [
        [
            (step, quarter)
            for step in range(steps)
            for quarter in ((0, 1, 2, 3), (2, 3, 0, 1))[way][: 4 if step < steps - 1 else 2]
        ]
        for way in range(2)
    ]
    chunk = width // QUARTERS
    moved = {"chunks": 0}

    def piece(ref, quarter):
        return ref.at[pl.ds(quarter * chunk, chunk)]

    def ring_copy(way, step, quarter):
        block = s["weights"].at[at(-step if way == 0 else step, core)]
        src = refs["weight"] if step == 0 else block
        index = (way * steps + step) * QUARTERS + quarter
        return remote(
            piece(src, quarter),
            piece(block, quarter),
            s["ring_send"].at[index],
            s["ring_recv"].at[index],
            dp=at(1 if way == 0 else -1, core),
        )

    def arrival(way, step, quarter, kind):
        offset = -1 - step if way == 0 else 1 + step
        here = s["weights"].at[at(offset, core if kind == "ring" else 1 - core)]
        here = piece(here, quarter)
        index = (way * steps + step) * QUARTERS + quarter
        peer = twin if kind == "twin" else at(1 if way == 0 else -1, core)
        return remote(
            here, here, s[kind + "_send"].at[index], s[kind + "_recv"].at[index], dp=peer
        )

    def twin_copy(way, step, quarter):
        offset = -1 - step if way == 0 else 1 + step
        here = piece(s["weights"].at[at(offset, core)], quarter)
        index = (way * steps + step) * QUARTERS + quarter
        return remote(here, here, s["twin_send"].at[index], s["twin_recv"].at[index], dp=twin)

    def twin_own(block):
        return remote(
            refs["weight"],
            s["weights"].at[block],
            s["twin_send"].at[2 * steps * QUARTERS],
            s["twin_recv"].at[2 * steps * QUARTERS],
            dp=twin,
        )

    def advance(count):
        count = min(count, len(order[0]))
        for place in range(moved["chunks"], count):
            for way in range(2):
                step, quarter = order[way][place]
                arrival(way, step, quarter, "ring").wait_recv()
                if (step + 1, quarter) in order[way]:
                    ring_copy(way, step + 1, quarter).start()
                twin_copy(way, step, quarter).start()
        moved["chunks"] = max(count, moved["chunks"])

    def start_weights():
        for place in range(QUARTERS if steps > 1 else 2):
            for way in range(2):
                ring_copy(way, *order[way][place]).start()
        twin_own(me_dp).start()
        s["weights"][me_dp] = refs["weight"][...]

    def wait_weights():
        advance(len(order[0]))
        twin_own(twin).wait_recv()
        for way in range(2):
            for place in order[way]:
                arrival(way, *place, "twin").wait_recv()

    def pair_at(i):
        offset = half + jnp.where(i % 2 == 1, -((i + 1) // 2), i // 2)
        return (me // 2 + offset) % pairs

    def squash():
        s["squashed"][...] = jnp.tanh(refs["decay_low"][...].astype(F32)).astype(BF16)
        fill_masks(s)

    def in_groups(first, count, size, body):
        size = math.gcd(count, size)

        @pl.loop(0, count // size)
        def _(i):
            body([pair_at(first + i * size + j) for j in range(size)])

    def prepare_half(first):
        in_groups(first, half, 4, lambda chosen: prepare_group(chosen, refs, s))

    def refine_half(first):
        chosen = [pair_at(jnp.int32(first + j)) for j in range(half)]
        heads = [2 * pair + h for pair in chosen for h in range(2)]

        @pl.loop(0, 6)
        def _(level):
            refine_group(heads, level, s)

    def message_copy(head):
        return remote(
            s["message"].at[head],
            s["got"].at[me],
            s["message_send"].at[head],
            s["message_recv"].at[me],
            sp=head,
        )

    def send_messages(chosen):
        for pair in chosen:
            for h in range(2):
                head = 2 * pair + h

                @pl.when(head != me)
                def _():
                    message_copy(head).start()

    def solve_half(first):
        size = math.gcd(half, 4)

        @pl.loop(0, half // size)
        def _(i):
            chosen = [pair_at(first + i * size + j) for j in range(size)]
            solve_group(chosen, refs, s)
            send_messages(chosen)

    low_half = lax.broadcasted_iota(jnp.int32, (HEAD, L), 1) < HEAD
    turn = lambda x: pltpu.roll(x, HEAD, 1)

    def unpack(n):
        both = s["got"][n, :HEAD].astype(F32)
        s["added"][n] = both
        s["moved"][n] = jnp.where(low_half, turn(both), 0.0).astype(BF16)
        parts = s["got"][n, HEAD:].astype(F32)
        s["kept"][n] = parts + turn(parts)

    def peer_at(j):
        offset = n_sp // 2 + jnp.where(j % 2 == 1, -((j + 1) // 2), j // 2)
        return (me + offset) % n_sp

    def unpack_all():
        s["got"][me] = s["message"][me]
        unpack(me)

        @pl.loop(0, n_sp - 1)
        def _(j):
            n = peer_at(j)
            remote(
                s["got"].at[n],
                s["got"].at[n],
                s["message_send"].at[n],
                s["message_recv"].at[n],
                sp=n,
            ).wait_recv()
            unpack(n)

    def state_copy(n):
        return remote(
            s["states"].at[n],
            s["starts"].at[me],
            s["state_send"].at[n],
            s["state_recv"].at[me],
            sp=n,
        )

    def on_state(state, x):
        high, low = split(x[HEAD:, :HEAD])
        left = rows(*split(state[:, :HEAD]))
        a = mm(left, high)
        return a[:HEAD] + a[HEAD:] + mm(left[:HEAD], low)

    def scan_all():
        spans = n_sp // SPAN
        row = lax.broadcasted_iota(jnp.int32, (2 * HEAD, L), 0)
        col = lax.broadcasted_iota(jnp.int32, (2 * HEAD, L), 1)
        start = (row == col + HEAD).astype(F32)
        xs = [start] * spans
        for j in range(SPAN):
            outs = []
            for g in range(spans):
                n = g * SPAN + j
                s["prefix"][n] = xs[g]
                outs.append(mm(rows(*split(xs[g][:, :HEAD])), s["moved"][n]))
            for g in range(spans):
                n = g * SPAN + j
                a = outs[g][: 2 * HEAD] + outs[g][2 * HEAD :]
                x = xs[g] * s["kept"][n][:1] - a
                xs[g] = rows(x[:HEAD] + s["added"][n], x[HEAD:])
        state = jnp.zeros((HEAD, HEAD), F32)
        for g in range(spans):
            s["entry"][g, :, :HEAD] = state
            if g + 1 < spans:
                state = on_state(state, xs[g]) + xs[g][:HEAD, :HEAD]

    def emit(n):
        x = s["prefix"][n]
        state = on_state(s["entry"][n // SPAN], x) + x[:HEAD, :HEAD]
        state = cols(state, state)
        s["states"][n] = jnp.where(
            low_half[: HEAD // 2], state[: HEAD // 2], state[HEAD // 2 :]
        ).astype(BF16)

    def emit_all():
        size = 4

        @pl.loop(0, n_sp // size)
        def _(i):
            for j in range(size):
                emit(peer_at(i * size + j))
            for j in range(size):
                n = peer_at(i * size + j)

                @pl.when(n != me)
                def _():
                    state_copy(n).start()

        s["starts"][me] = s["states"][me]

    def local_all():
        in_groups(0, pairs, 4, lambda chosen: local_group(chosen, refs, s))

    def wait_starts():
        @pl.loop(0, n_sp - 1)
        def _(j):
            n = peer_at(j)
            remote(
                s["starts"].at[n],
                s["starts"].at[n],
                s["state_send"].at[n],
                s["state_recv"].at[n],
                sp=n,
            ).wait_recv()

    def read_all():
        in_groups(0, pairs, 4, lambda chosen: read_group(chosen, refs, s))

    def project():
        @pl.loop(0, n_dp // 2)
        def _(i):
            both = cols(s["weights"][2 * i], s["weights"][2 * i + 1])
            out[:, pl.ds(pl.multiple_of(i * 2 * L, 2 * L), 2 * L)] = mm(
                s["mix"][...], both
            ).astype(BF16)

    def drain():
        twin_own(me_dp).wait_send()
        for way in range(2):
            for place in order[way]:
                ring_copy(way, *place).wait_send()
                twin_copy(way, *place).wait_send()

        @pl.loop(1, n_sp)
        def _(j):
            n = (me + j) % n_sp
            message_copy(n).wait_send()
            state_copy(n).wait_send()

    phases = [
        ("greet", greet),
        ("squash", squash),
        ("met", met),
        ("weights", start_weights),
        ("prepare0", functools.partial(prepare_half, 0)),
        ("refine0", functools.partial(refine_half, 0)),
        ("solve0", functools.partial(solve_half, 0)),
        ("prepare1", functools.partial(prepare_half, half)),
        ("refine1", functools.partial(refine_half, half)),
        ("solve1", functools.partial(solve_half, half)),
        ("unpack", unpack_all),
        ("scan", scan_all),
        ("emit", emit_all),
        ("local", local_all),
        ("starts", wait_starts),
        ("read", read_all),
        ("whole", wait_weights),
        ("project", project),
        ("drain", drain),
    ]
    for name, phase in phases:
        with jax.named_scope(name):
            phase()
        if name in schedule:
            with jax.named_scope("pass_" + name):
                advance(schedule[name])


SCHEDULE = {
    "prepare0": 1,
    "refine0": 2,
    "solve0": 3,
    "prepare1": 4,
    "refine1": 6,
    "solve1": 7,
    "unpack": 8,
    "emit": 9,
    "local": 10,
    "starts": 12,
}


def solution(mesh):
    n_sp, n_dp = mesh.shape["sp"], mesh.shape["dp"]

    def per_device(
        query_rows,
        key_rows,
        value_rows,
        decay_low,
        rate_low,
        decay_up,
        rate_up,
        decay_base,
        norm_gain,
        out_weight,
    ):
        width = query_rows.shape[2]
        vmem = pl.BlockSpec(memory_space=pltpu.VMEM)
        out = pl.pallas_call(
            functools.partial(
                whole_kernel, n_sp=n_sp, n_dp=n_dp, width=width, schedule=SCHEDULE
            ),
            out_shape=jax.ShapeDtypeStruct((L, n_dp * L), BF16),
            in_specs=[vmem] * len(INPUTS),
            out_specs=vmem,
            scratch_shapes=list(scratch(width, n_sp, n_dp).values()),
            compiler_params=pltpu.CompilerParams(
                collective_id=0, has_side_effects=True, vmem_limit_bytes=60 * 2**20
            ),
            name="mixer",
        )(
            query_rows[0],
            key_rows[0],
            value_rows[0],
            decay_low[0],
            rate_low[0],
            decay_up,
            rate_up,
            decay_base[None],
            norm_gain[None],
            out_weight,
        )
        return out[None]

    rows_spec = P("dp", "sp", None)
    return jax.shard_map(
        per_device,
        mesh=mesh,
        in_specs=(rows_spec,) * 5 + (P(), P(), P(), P(), P(None, "dp")),
        out_specs=rows_spec,
        check_vma=False,
    )
```

time: 93.9 us -> 68 us (0.72)
  Pallas kernels: 91.3 us -> 65.9 us
    pallas_call x1, Pallas kernels: 91.3 us -> 65.9 us  [per_device(): pl.pallas_call(functools.partial(whole_kernel, n_sp=n_sp, n_dp=n_dp, widt...]
where the time goes in v2:
time: 68 us; the launch traced here: 67.8 us
  Pallas kernels  65.9 us (97%)
  local copies, waits for them, and re-layouts  1.88 us (3%)
    pallas_call x1, Pallas kernels, per_device(): pl.pallas_call(functools.partial(whole_kernel, n_sp=n_sp, n_dp=n_dp, widt...  65.9 us
    unnamed x1, local copies, waits for them, and re-layouts  1.88 us

profile of v2, /device:TPU:1, one launch (start us, length us, event | category | flops | bytes accessed | tf_op | source)
XLA Modules:
  0.0 67.8 jit_solution(14123008319785719376)
XLA Ops:
  0.0 65.9 %mixer.1 = bf16[128,2048]{1,0:T(8,128)(2,1)} custom-call(bf16[128,2048]{1,0:T(8,128)(2,1)} %bitcast.9, bf16[128,2048]{1,0:T(8,128)(2,1)} %bitcast.10, bf16[128,2048]{1,0:T(8,128)(2,1)} %bitcast.11, bf16[128,128]{1,0:T(8,128)(2,1)} %bitcast.12, bf16[128,128]{1,0:T(8,128)(2,1)} %bitcast.13, bf16[128,2048]{1,0:T(8,128)(2,1)} %args_5_.4, ...), custom_call_target="tpu_custom_call" | custom-call | tf_op jit(solution)/shard_map/mixer/pallas_call | solution.py:659
  65.9 1.9 %copy.12 = bf16[1,128,2048]{2,1,0:T(8,128)(2,1)} copy(bf16[1,128,2048]{2,1,0:T(8,128)(2,1)} %bitcast.8) | data formatting | bytes 1048576

commit v3 on v2

--- a/solution.py
+++ b/solution.py
@@ -16,6 +16,8 @@
 MSG = HEAD + TAIL
 QUARTERS = 4
 SPAN = 4
+SHARED = 3
+ALONG_X = 4
 
 
 def split(x):
@@ -257,6 +259,20 @@
     )
 
 
+INPUTS = (
+    "query",
+    "key",
+    "value",
+    "decay_low",
+    "rate_low",
+    "decay_up",
+    "rate_up",
+    "base",
+    "gain",
+    "weight",
+)
+
+
 def scratch(width, n_sp, n_dp):
     made = local_scratch(width)
     heads = width // HEAD
@@ -276,6 +292,18 @@
         starts=pltpu.VMEM((heads, HEAD // 2, L), BF16),
         mix=pltpu.VMEM((L, width), BF16),
         weights=pltpu.VMEM((n_dp, width, L), BF16),
+        query=pltpu.VMEM((L, width), BF16),
+        key=pltpu.VMEM((L, width), BF16),
+        value=pltpu.VMEM((L, width), BF16),
+        decay_low=pltpu.VMEM((L, L), BF16),
+        rate_low=pltpu.VMEM((L, L), BF16),
+        decay_up=pltpu.VMEM((L, width), BF16),
+        rate_up=pltpu.VMEM((L, width), BF16),
+        base=pltpu.VMEM((1, width), F32),
+        gain=pltpu.VMEM((1, width), F32),
+        fetched=dma((len(INPUTS),)),
+        x_send=dma((2 * chunks,)),
+        x_recv=dma((2 * chunks,)),
         message_send=dma((n_sp,)),
         message_recv=dma((n_sp,)),
         state_send=dma((n_sp,)),
@@ -288,18 +316,6 @@
     return made
 
 
-INPUTS = (
-    "query",
-    "key",
-    "value",
-    "decay_low",
-    "rate_low",
-    "decay_up",
-    "rate_up",
-    "base",
-    "gain",
-    "weight",
-)
 MESH = pl.DeviceIdType.MESH
 
 
@@ -310,9 +326,10 @@
 
 
 def whole_kernel(*args, n_sp, n_dp, width, schedule):
-    refs = dict(zip(INPUTS, args))
+    given = dict(zip(INPUTS, args))
     out = args[len(INPUTS)]
     s = dict(zip(scratch(width, n_sp, n_dp), args[len(INPUTS) + 1 :]))
+    refs = {name: s[name] for name in INPUTS if name != "weight"}
     pairs = width // L
     half = pairs // 2
     me = lax.axis_index("sp")
@@ -321,7 +338,19 @@
     steps = ring // 2
     twin = y * 2 + 1 - core
     at = lambda offset, c: ((y + offset + ring) % ring) * 2 + c
+    along = math.gcd(n_sp, ALONG_X)
+    x = me % along
     barrier = pltpu.get_barrier_semaphore()
+
+    def fetch(name):
+        target = s["weights"].at[me_dp] if name == "weight" else s[name]
+        return pltpu.make_async_copy(given[name], target, s["fetched"].at[INPUTS.index(name)])
+
+    def fetch_all():
+        for name in ("decay_low", "decay_up", "base", "rate_low", "rate_up", "key", "query"):
+            fetch(name).start()
+        for name in ("value", "gain", "weight"):
+            fetch(name).start()
 
     def greet():
         @pl.loop(1, n_sp)
@@ -340,19 +369,30 @@
         [
             (step, quarter)
             for step in range(steps)
-            for quarter in ((0, 1, 2, 3), (2, 3, 0, 1))[way][: 4 if step < steps - 1 else 2]
+            for quarter in (
+                ((SHARED, 0, 1, 2), (SHARED, 2, 0, 1))[way]
+                if step < steps - 1
+                else ((0, 1), (SHARED, 2))[way]
+            )
         ]
         for way in range(2)
     ]
     chunk = width // QUARTERS
     moved = {"chunks": 0}
 
+    share = chunk // along
+
     def piece(ref, quarter):
+        if quarter != SHARED:
+            return ref.at[pl.ds(quarter * chunk, chunk)]
+        return ref.at[pl.ds(pl.multiple_of(SHARED * chunk + x * share, share), share)]
+
+    def whole_piece(ref, quarter):
         return ref.at[pl.ds(quarter * chunk, chunk)]
 
     def ring_copy(way, step, quarter):
         block = s["weights"].at[at(-step if way == 0 else step, core)]
-        src = refs["weight"] if step == 0 else block
+        src = given["weight"] if step == 0 else block
         index = (way * steps + step) * QUARTERS + quarter
         return remote(
             piece(src, quarter),
@@ -365,7 +405,7 @@
     def arrival(way, step, quarter, kind):
         offset = -1 - step if way == 0 else 1 + step
         here = s["weights"].at[at(offset, core if kind == "ring" else 1 - core)]
-        here = piece(here, quarter)
+        here = (piece if kind == "ring" else whole_piece)(here, quarter)
         index = (way * steps + step) * QUARTERS + quarter
         peer = twin if kind == "twin" else at(1 if way == 0 else -1, core)
         return remote(
@@ -374,18 +414,33 @@
 
     def twin_copy(way, step, quarter):
         offset = -1 - step if way == 0 else 1 + step
-        here = piece(s["weights"].at[at(offset, core)], quarter)
+        here = whole_piece(s["weights"].at[at(offset, core)], quarter)
         index = (way * steps + step) * QUARTERS + quarter
         return remote(here, here, s["twin_send"].at[index], s["twin_recv"].at[index], dp=twin)
 
     def twin_own(block):
         return remote(
-            refs["weight"],
+            given["weight"],
             s["weights"].at[block],
             s["twin_send"].at[2 * steps * QUARTERS],
             s["twin_recv"].at[2 * steps * QUARTERS],
             dp=twin,
         )
+
+    def x_copy(way, step, k, theirs=False):
+        offset = -1 - step if way == 0 else 1 + step
+        start = SHARED * chunk + ((x - k + along) % along if theirs else x) * share
+        here = s["weights"].at[at(offset, core)]
+        here = here.at[pl.ds(pl.multiple_of(start, share), share)]
+        index = (way * steps + step) * QUARTERS + k
+        return remote(
+            here, here, s["x_send"].at[index], s["x_recv"].at[index], sp=me - x + (x + k) % along
+        )
+
+    def join(way, step):
+        for k in range(1, along):
+            x_copy(way, step, k, True).wait_recv()
+        twin_copy(way, step, SHARED).start()
 
     def advance(count):
         count = min(count, len(order[0]))
@@ -395,7 +450,17 @@
                 arrival(way, step, quarter, "ring").wait_recv()
                 if (step + 1, quarter) in order[way]:
                     ring_copy(way, step + 1, quarter).start()
-                twin_copy(way, step, quarter).start()
+                if quarter == SHARED:
+                    for k in range(1, along):
+                        x_copy(way, step, k).start()
+                    moved[(way, step)] = place + 2
+                else:
+                    twin_copy(way, step, quarter).start()
+            for way in range(2):
+                for step in range(steps):
+                    if moved.get((way, step)) == place:
+                        join(way, step)
+                        moved[(way, step)] = -1
         moved["chunks"] = max(count, moved["chunks"])
 
     def start_weights():
@@ -403,22 +468,39 @@
             for way in range(2):
                 ring_copy(way, *order[way][place]).start()
         twin_own(me_dp).start()
-        s["weights"][me_dp] = refs["weight"][...]
-
-    def wait_weights():
-        advance(len(order[0]))
+
+    def project_at(offset):
+        both = cols(s["weights"][at(offset, 0)], s["weights"][at(offset, 1)])
+        where = pl.ds(pl.multiple_of(at(offset, 0) * L, 2 * L), 2 * L)
+        out[:, where] = mm(s["mix"][...], both).astype(BF16)
+
+    def project():
+        fetch("weight").wait()
         twin_own(twin).wait_recv()
-        for way in range(2):
-            for place in order[way]:
-                arrival(way, *place, "twin").wait_recv()
+        project_at(0)
+        for step in range(steps):
+            advance(QUARTERS * (step + 1) + 3)
+            for way in range(2):
+                if moved.get((way, step), -1) >= 0:
+                    join(way, step)
+                    moved[(way, step)] = -1
+            for way in range(2):
+                for place in order[way]:
+                    if place[0] == step:
+                        arrival(way, *place, "twin").wait_recv()
+                if step < steps - 1 or way == 1:
+                    project_at(-1 - step if way == 0 else 1 + step)
 
     def pair_at(i):
         offset = half + jnp.where(i % 2 == 1, -((i + 1) // 2), i // 2)
         return (me // 2 + offset) % pairs
 
     def squash():
+        fetch("decay_low").wait()
         s["squashed"][...] = jnp.tanh(refs["decay_low"][...].astype(F32)).astype(BF16)
         fill_masks(s)
+        for name in ("decay_up", "base", "rate_low", "rate_up", "key", "query"):
+            fetch(name).wait()
 
     def in_groups(first, count, size, body):
         size = math.gcd(count, size)
@@ -457,6 +539,9 @@
                     message_copy(head).start()
 
     def solve_half(first):
+        if first == 0:
+            fetch("value").wait()
+            fetch("gain").wait()
         size = math.gcd(half, 4)
 
         @pl.loop(0, half // size)
@@ -481,7 +566,6 @@
 
     def unpack_all():
         s["got"][me] = s["message"][me]
-        unpack(me)
 
         @pl.loop(0, n_sp - 1)
         def _(j):
@@ -493,7 +577,13 @@
                 s["message_recv"].at[n],
                 sp=n,
             ).wait_recv()
-            unpack(n)
+
+        size = math.gcd(n_sp, 8)
+
+        @pl.loop(0, n_sp // size)
+        def _(i):
+            for j in range(size):
+                unpack(i * size + j)
 
     def state_copy(n):
         return remote(
@@ -542,7 +632,7 @@
         ).astype(BF16)
 
     def emit_all():
-        size = 4
+        size = math.gcd(n_sp, 8)
 
         @pl.loop(0, n_sp // size)
         def _(i):
@@ -575,20 +665,15 @@
     def read_all():
         in_groups(0, pairs, 4, lambda chosen: read_group(chosen, refs, s))
 
-    def project():
-        @pl.loop(0, n_dp // 2)
-        def _(i):
-            both = cols(s["weights"][2 * i], s["weights"][2 * i + 1])
-            out[:, pl.ds(pl.multiple_of(i * 2 * L, 2 * L), 2 * L)] = mm(
-                s["mix"][...], both
-            ).astype(BF16)
-
     def drain():
         twin_own(me_dp).wait_send()
         for way in range(2):
             for place in order[way]:
                 ring_copy(way, *place).wait_send()
                 twin_copy(way, *place).wait_send()
+                if place[1] == SHARED:
+                    for k in range(1, along):
+                        x_copy(way, place[0], k).wait_send()
 
         @pl.loop(1, n_sp)
         def _(j):
@@ -598,9 +683,10 @@
 
     phases = [
         ("greet", greet),
-        ("squash", squash),
+        ("fetch", fetch_all),
         ("met", met),
         ("weights", start_weights),
+        ("squash", squash),
         ("prepare0", functools.partial(prepare_half, 0)),
         ("refine0", functools.partial(refine_half, 0)),
         ("solve0", functools.partial(solve_half, 0)),
@@ -613,7 +699,6 @@
         ("local", local_all),
         ("starts", wait_starts),
         ("read", read_all),
-        ("whole", wait_weights),
         ("project", project),
         ("drain", drain),
     ]
@@ -629,12 +714,12 @@
     "prepare0": 1,
     "refine0": 2,
     "solve0": 3,
-    "prepare1": 4,
+    "prepare1": 5,
     "refine1": 6,
     "solve1": 7,
-    "unpack": 8,
-    "emit": 9,
-    "local": 10,
+    "unpack": 9,
+    "emit": 10,
+    "local": 11,
     "starts": 12,
 }
 
@@ -656,12 +741,13 @@
     ):
         width = query_rows.shape[2]
         vmem = pl.BlockSpec(memory_space=pltpu.VMEM)
+        hbm = pl.BlockSpec(memory_space=pl.ANY)
         out = pl.pallas_call(
             functools.partial(
                 whole_kernel, n_sp=n_sp, n_dp=n_dp, width=width, schedule=SCHEDULE
             ),
             out_shape=jax.ShapeDtypeStruct((L, n_dp * L), BF16),
-            in_specs=[vmem] * len(INPUTS),
+            in_specs=[hbm] * len(INPUTS),
             out_specs=vmem,
             scratch_shapes=list(scratch(width, n_sp, n_dp).values()),
             compiler_params=pltpu.CompilerParams(

time: 68 us -> 68.1 us (level)
  no operation moved by 1% of the time
where the time goes in v3:
time: 68.1 us; the launch traced here: 68 us
  Pallas kernels  66.1 us (97%)
  local copies, waits for them, and re-layouts  1.88 us (3%)
    pallas_call x1, Pallas kernels, per_device(): pl.pallas_call(functools.partial(whole_kernel, n_sp=n_sp, n_dp=n_dp, widt...  66.1 us
    unnamed x1, local copies, waits for them, and re-layouts  1.88 us

profile of v3, /device:TPU:1, one launch (start us, length us, event | category | flops | bytes accessed | tf_op | source)
XLA Modules:
  0.0 68.0 jit_solution(7831087433228601119)
XLA Ops:
  0.0 66.1 %mixer.1 = bf16[128,2048]{1,0:T(8,128)(2,1)} custom-call(bf16[128,2048]{1,0:T(8,128)(2,1)} %bitcast.9, bf16[128,2048]{1,0:T(8,128)(2,1)} %bitcast.10, bf16[128,2048]{1,0:T(8,128)(2,1)} %bitcast.11, bf16[128,128]{1,0:T(8,128)(2,1)} %bitcast.12, bf16[128,128]{1,0:T(8,128)(2,1)} %bitcast.13, bf16[128,2048]{1,0:T(8,128)(2,1)} %args_5_.4, ...), custom_call_target="tpu_custom_call" | custom-call | tf_op jit(solution)/shard_map/mixer/pallas_call | solution.py:745
  66.1 1.9 %copy.12 = bf16[1,128,2048]{2,1,0:T(8,128)(2,1)} copy(bf16[1,128,2048]{2,1,0:T(8,128)(2,1)} %bitcast.8) | data formatting | bytes 1048576

commit v4 on v3

--- a/solution.py
+++ b/solution.py
@@ -302,16 +302,16 @@
         base=pltpu.VMEM((1, width), F32),
         gain=pltpu.VMEM((1, width), F32),
         fetched=dma((len(INPUTS),)),
-        x_send=dma((2 * chunks,)),
-        x_recv=dma((2 * chunks,)),
-        message_send=dma((n_sp,)),
-        message_recv=dma((n_sp,)),
-        state_send=dma((n_sp,)),
-        state_recv=dma((n_sp,)),
-        ring_send=dma((2 * chunks,)),
+        x_send=dma,
+        x_recv=dma((n_dp // 2,)),
+        message_send=dma,
+        message_recv=dma,
+        state_send=dma,
+        state_recv=dma,
+        ring_send=dma,
         ring_recv=dma((2 * chunks,)),
-        twin_send=dma((2 * chunks + 1,)),
-        twin_recv=dma((2 * chunks + 1,)),
+        twin_send=dma,
+        twin_recv=dma((n_dp // 2,)),
     )
     return made
 
@@ -332,6 +332,7 @@
     refs = {name: s[name] for name in INPUTS if name != "weight"}
     pairs = width // L
     half = pairs // 2
+    early = max(1, pairs // 4)
     me = lax.axis_index("sp")
     me_dp = lax.axis_index("dp")
     core, y, ring = me_dp % 2, me_dp // 2, n_dp // 2
@@ -372,7 +373,7 @@
             for quarter in (
                 ((SHARED, 0, 1, 2), (SHARED, 2, 0, 1))[way]
                 if step < steps - 1
-                else ((0, 1), (SHARED, 2))[way]
+                else ((0, 1), (2, SHARED))[way]
             )
         ]
         for way in range(2)
@@ -390,67 +391,71 @@
     def whole_piece(ref, quarter):
         return ref.at[pl.ds(quarter * chunk, chunk)]
 
+    def spot(way, step):
+        return 2 * step + (way if step < steps - 1 else 0)
+
     def ring_copy(way, step, quarter):
         block = s["weights"].at[at(-step if way == 0 else step, core)]
         src = given["weight"] if step == 0 else block
-        index = (way * steps + step) * QUARTERS + quarter
+        cut = piece if step < steps - 1 else whole_piece
         return remote(
-            piece(src, quarter),
-            piece(block, quarter),
-            s["ring_send"].at[index],
-            s["ring_recv"].at[index],
+            cut(src, quarter),
+            cut(block, quarter),
+            s["ring_send"],
+            s["ring_recv"].at[(way * steps + step) * QUARTERS + quarter],
             dp=at(1 if way == 0 else -1, core),
         )
 
-    def arrival(way, step, quarter, kind):
-        offset = -1 - step if way == 0 else 1 + step
-        here = s["weights"].at[at(offset, core if kind == "ring" else 1 - core)]
-        here = (piece if kind == "ring" else whole_piece)(here, quarter)
-        index = (way * steps + step) * QUARTERS + quarter
-        peer = twin if kind == "twin" else at(1 if way == 0 else -1, core)
-        return remote(
-            here, here, s[kind + "_send"].at[index], s[kind + "_recv"].at[index], dp=peer
-        )
+    def arrival(way, step, quarter):
+        here = s["weights"].at[at(-1 - step if way == 0 else 1 + step, core)]
+        here = (piece if step < steps - 1 else whole_piece)(here, quarter)
+        recv = s["ring_recv"].at[(way * steps + step) * QUARTERS + quarter]
+        return remote(here, here, s["ring_send"], recv, dp=at(1 if way == 0 else -1, core))
 
     def twin_copy(way, step, quarter):
-        offset = -1 - step if way == 0 else 1 + step
-        here = whole_piece(s["weights"].at[at(offset, core)], quarter)
-        index = (way * steps + step) * QUARTERS + quarter
-        return remote(here, here, s["twin_send"].at[index], s["twin_recv"].at[index], dp=twin)
+        here = s["weights"].at[at(-1 - step if way == 0 else 1 + step, core)]
+        here = whole_piece(here, quarter)
+        return remote(here, here, s["twin_send"], s["twin_recv"].at[spot(way, step)], dp=twin)
+
+    def twin_block(way, step):
+        here = s["weights"].at[at(-1 - step if way == 0 else 1 + step, 1 - core)]
+        return remote(here, here, s["twin_send"], s["twin_recv"].at[spot(way, step)], dp=twin)
 
     def twin_own(block):
         return remote(
             given["weight"],
             s["weights"].at[block],
-            s["twin_send"].at[2 * steps * QUARTERS],
-            s["twin_recv"].at[2 * steps * QUARTERS],
+            s["twin_send"],
+            s["twin_recv"].at[2 * steps - 1],
             dp=twin,
         )
 
-    def x_copy(way, step, k, theirs=False):
-        offset = -1 - step if way == 0 else 1 + step
-        start = SHARED * chunk + ((x - k + along) % along if theirs else x) * share
-        here = s["weights"].at[at(offset, core)]
-        here = here.at[pl.ds(pl.multiple_of(start, share), share)]
-        index = (way * steps + step) * QUARTERS + k
-        return remote(
-            here, here, s["x_send"].at[index], s["x_recv"].at[index], sp=me - x + (x + k) % along
-        )
+    def x_copy(way, step, k):
+        here = piece(s["weights"].at[at(-1 - step if way == 0 else 1 + step, core)], SHARED)
+        peer = me - x + (x + k) % along
+        return remote(here, here, s["x_send"], s["x_recv"].at[spot(way, step)], sp=peer)
+
+    def sent(kind, count):
+        here = s["weights"].at[:, pl.ds(0, count // n_dp)]
+        return remote(here, here, s[kind + "_send"], s["twin_recv"].at[0], dp=twin)
 
     def join(way, step):
-        for k in range(1, along):
-            x_copy(way, step, k, True).wait_recv()
+        here = s["weights"].at[me_dp, pl.ds(0, share * (along - 1))]
+        remote(here, here, s["x_send"], s["x_recv"].at[spot(way, step)], dp=twin).wait_recv()
         twin_copy(way, step, SHARED).start()
+        if step == steps - 2 and (step + 1, SHARED) in order[way]:
+            ring_copy(way, step + 1, SHARED).start()
 
     def advance(count):
         count = min(count, len(order[0]))
         for place in range(moved["chunks"], count):
             for way in range(2):
                 step, quarter = order[way][place]
-                arrival(way, step, quarter, "ring").wait_recv()
-                if (step + 1, quarter) in order[way]:
+                arrival(way, step, quarter).wait_recv()
+                parted = quarter == SHARED and step < steps - 1
+                if (step + 1, quarter) in order[way] and not (parted and step == steps - 2):
                     ring_copy(way, step + 1, quarter).start()
-                if quarter == SHARED:
+                if parted:
                     for k in range(1, along):
                         x_copy(way, step, k).start()
                     moved[(way, step)] = place + 2
@@ -485,10 +490,8 @@
                     join(way, step)
                     moved[(way, step)] = -1
             for way in range(2):
-                for place in order[way]:
-                    if place[0] == step:
-                        arrival(way, *place, "twin").wait_recv()
                 if step < steps - 1 or way == 1:
+                    twin_block(way, step).wait_recv()
                     project_at(-1 - step if way == 0 else 1 + step)
 
     def pair_at(i):
@@ -509,14 +512,14 @@
         def _(i):
             body([pair_at(first + i * size + j) for j in range(size)])
 
-    def prepare_half(first):
-        in_groups(first, half, 4, lambda chosen: prepare_group(chosen, refs, s))
-
-    def refine_half(first):
-        chosen = [pair_at(jnp.int32(first + j)) for j in range(half)]
+    def prepare_part(first, count):
+        in_groups(first, count, 4, lambda chosen: prepare_group(chosen, refs, s))
+
+    def refine_part(first, count, low, high):
+        chosen = [pair_at(jnp.int32(first + j)) for j in range(count)]
         heads = [2 * pair + h for pair in chosen for h in range(2)]
 
-        @pl.loop(0, 6)
+        @pl.loop(low, high)
         def _(level):
             refine_group(heads, level, s)
 
@@ -524,8 +527,8 @@
         return remote(
             s["message"].at[head],
             s["got"].at[me],
-            s["message_send"].at[head],
-            s["message_recv"].at[me],
+            s["message_send"],
+            s["message_recv"],
             sp=head,
         )
 
@@ -538,13 +541,13 @@
                 def _():
                     message_copy(head).start()
 
-    def solve_half(first):
+    def solve_part(first, count):
         if first == 0:
             fetch("value").wait()
             fetch("gain").wait()
-        size = math.gcd(half, 4)
-
-        @pl.loop(0, half // size)
+        size = math.gcd(count, 4)
+
+        @pl.loop(0, count // size)
         def _(i):
             chosen = [pair_at(first + i * size + j) for j in range(size)]
             solve_group(chosen, refs, s)
@@ -564,20 +567,14 @@
         offset = n_sp // 2 + jnp.where(j % 2 == 1, -((j + 1) // 2), j // 2)
         return (me + offset) % n_sp
 
+    def all_of(name, kind):
+        rest = s[name].at[pl.ds(0, n_sp - 1)]
+        return remote(rest, rest, s[kind + "_send"], s[kind + "_recv"], sp=(me + 1) % n_sp)
+
     def unpack_all():
         s["got"][me] = s["message"][me]
 
-        @pl.loop(0, n_sp - 1)
-        def _(j):
-            n = peer_at(j)
-            remote(
-                s["got"].at[n],
-                s["got"].at[n],
-                s["message_send"].at[n],
-                s["message_recv"].at[n],
-                sp=n,
-            ).wait_recv()
-
+        all_of("got", "message").wait_recv()
         size = math.gcd(n_sp, 8)
 
         @pl.loop(0, n_sp // size)
@@ -589,8 +586,8 @@
         return remote(
             s["states"].at[n],
             s["starts"].at[me],
-            s["state_send"].at[n],
-            s["state_recv"].at[me],
+            s["state_send"],
+            s["state_recv"],
             sp=n,
         )
 
@@ -650,36 +647,21 @@
     def local_all():
         in_groups(0, pairs, 4, lambda chosen: local_group(chosen, refs, s))
 
+        all_of("message", "message").wait_send()
+
     def wait_starts():
-        @pl.loop(0, n_sp - 1)
-        def _(j):
-            n = peer_at(j)
-            remote(
-                s["starts"].at[n],
-                s["starts"].at[n],
-                s["state_send"].at[n],
-                s["state_recv"].at[n],
-                sp=n,
-            ).wait_recv()
+        all_of("starts", "state").wait_recv()
 
     def read_all():
         in_groups(0, pairs, 4, lambda chosen: read_group(chosen, refs, s))
 
     def drain():
-        twin_own(me_dp).wait_send()
-        for way in range(2):
-            for place in order[way]:
-                ring_copy(way, *place).wait_send()
-                twin_copy(way, *place).wait_send()
-                if place[1] == SHARED:
-                    for k in range(1, along):
-                        x_copy(way, place[0], k).wait_send()
-
-        @pl.loop(1, n_sp)
-        def _(j):
-            n = (me + j) % n_sp
-            message_copy(n).wait_send()
-            state_copy(n).wait_send()
+        ringed = (steps - 1) * (3 * chunk + share) + 2 * chunk
+        sent("ring", 2 * ringed).wait_send()
+        sent("x", 2 * (steps - 1) * (along - 1) * share).wait_send()
+        whole = s["weights"].at[pl.ds(0, n_dp // 2)]
+        remote(whole, whole, s["twin_send"], s["twin_recv"].at[0], dp=twin).wait_send()
+        all_of("states", "state").wait_send()
 
     phases = [
         ("greet", greet),
@@ -687,12 +669,14 @@
         ("met", met),
         ("weights", start_weights),
         ("squash", squash),
-        ("prepare0", functools.partial(prepare_half, 0)),
-        ("refine0", functools.partial(refine_half, 0)),
-        ("solve0", functools.partial(solve_half, 0)),
-        ("prepare1", functools.partial(prepare_half, half)),
-        ("refine1", functools.partial(refine_half, half)),
-        ("solve1", functools.partial(solve_half, half)),
+        ("prepare0", functools.partial(prepare_part, 0, early)),
+        ("refine0a", functools.partial(refine_part, 0, early, 0, 3)),
+        ("refine0b", functools.partial(refine_part, 0, early, 3, 6)),
+        ("solve0", functools.partial(solve_part, 0, early)),
+        ("prepare1", functools.partial(prepare_part, early, pairs - early)),
+        ("refine1a", functools.partial(refine_part, early, pairs - early, 0, 3)),
+        ("refine1b", functools.partial(refine_part, early, pairs - early, 3, 6)),
+        ("solve1", functools.partial(solve_part, early, pairs - early)),
         ("unpack", unpack_all),
         ("scan", scan_all),
         ("emit", emit_all),
@@ -711,16 +695,15 @@
 
 
 SCHEDULE = {
-    "prepare0": 1,
-    "refine0": 2,
-    "solve0": 3,
-    "prepare1": 5,
-    "refine1": 6,
-    "solve1": 7,
+    "prepare1": 2,
+    "refine1a": 3,
+    "refine1b": 4,
+    "solve1": 6,
     "unpack": 9,
     "emit": 10,
     "local": 11,
     "starts": 12,
+    "read": 13,
 }
 
 
@@ -746,7 +729,7 @@
             functools.partial(
                 whole_kernel, n_sp=n_sp, n_dp=n_dp, width=width, schedule=SCHEDULE
             ),
-            out_shape=jax.ShapeDtypeStruct((L, n_dp * L), BF16),
+            out_shape=pltpu.VMEM((L, n_dp * L), BF16),
             in_specs=[hbm] * len(INPUTS),
             out_specs=vmem,
             scratch_shapes=list(scratch(width, n_sp, n_dp).values()),

time: 68.1 us -> 64.1 us (0.941)
  Pallas kernels: 66.1 us -> 63.2 us
  local copies, waits for them, and re-layouts: 1.88 us -> 0.8 us
    pallas_call x1, Pallas kernels: 66.1 us -> 63.2 us  [per_device(): pl.pallas_call(functools.partial(whole_kernel, n_sp=n_sp, n_dp=n_dp, widt...]
    unnamed x1, local copies, waits for them, and re-layouts: 1.88 us -> 0.8 us
where the time goes in v4:
time: 64.1 us; the launch traced here: 64 us
  Pallas kernels  63.2 us (99%)
  local copies, waits for them, and re-layouts  0.8 us (1%)
    pallas_call x1, Pallas kernels, per_device(): pl.pallas_call(functools.partial(whole_kernel, n_sp=n_sp, n_dp=n_dp, widt...  63.2 us

profile of v4, /device:TPU:1, one launch (start us, length us, event | category | flops | bytes accessed | tf_op | source)
XLA Modules:
  0.0 64.0 jit_solution(17120504902888762568)
XLA Ops:
  0.0 63.2 %mixer.1 = bf16[128,2048]{1,0:T(8,128)(2,1)S(1)} custom-call(bf16[128,2048]{1,0:T(8,128)(2,1)} %bitcast.9, bf16[128,2048]{1,0:T(8,128)(2,1)} %bitcast.10, bf16[128,2048]{1,0:T(8,128)(2,1)} %bitcast.11, bf16[128,128]{1,0:T(8,128)(2,1)} %bitcast.12, bf16[128,128]{1,0:T(8,128)(2,1)} %bitcast.13, bf16[128,2048]{1,0:T(8,128)(2,1)} %args_5_.4, ...), custom_call_target="tpu_custom_call" | custom-call | tf_op jit(solution)/shard_map/mixer/pallas_call | solution.py:728
  63.2 0.8 %copy.12 = bf16[1,128,2048]{2,1,0:T(8,128)(2,1)} copy(bf16[1,128,2048]{2,1,0:T(8,128)(2,1)S(1)} %bitcast.8) | data formatting | bytes 1048576

commit v5 on v4

--- a/solution.py
+++ b/solution.py
@@ -332,7 +332,7 @@
     refs = {name: s[name] for name in INPUTS if name != "weight"}
     pairs = width // L
     half = pairs // 2
-    early = max(1, pairs // 4)
+    early = half
     me = lax.axis_index("sp")
     me_dp = lax.axis_index("dp")
     core, y, ring = me_dp % 2, me_dp // 2, n_dp // 2
@@ -695,11 +695,12 @@
 
 
 SCHEDULE = {
-    "prepare1": 2,
-    "refine1a": 3,
-    "refine1b": 4,
+    "solve0": 2,
+    "prepare1": 3,
+    "refine1b": 5,
     "solve1": 6,
-    "unpack": 9,
+    "unpack": 8,
+    "scan": 9,
     "emit": 10,
     "local": 11,
     "starts": 12,

time: 64.1 us -> 61 us (0.952)
  Pallas kernels: 63.2 us -> 60.1 us
    pallas_call x1, Pallas kernels: 63.2 us -> 60.1 us  [per_device(): pl.pallas_call(functools.partial(whole_kernel, n_sp=n_sp, n_dp=n_dp, widt...]
where the time goes in v5:
time: 61 us; the launch traced here: 60.9 us
  Pallas kernels  60.1 us (99%)
  local copies, waits for them, and re-layouts  0.8 us (1%)
    pallas_call x1, Pallas kernels, per_device(): pl.pallas_call(functools.partial(whole_kernel, n_sp=n_sp, n_dp=n_dp, widt...  60.1 us

profile of v5, /device:TPU:1, one launch (start us, length us, event | category | flops | bytes accessed | tf_op | source)
XLA Modules:
  0.0 60.9 jit_solution(18392126752626107572)
XLA Ops:
  0.0 60.1 %mixer.1 = bf16[128,2048]{1,0:T(8,128)(2,1)S(1)} custom-call(bf16[128,2048]{1,0:T(8,128)(2,1)} %bitcast.9, bf16[128,2048]{1,0:T(8,128)(2,1)} %bitcast.10, bf16[128,2048]{1,0:T(8,128)(2,1)} %bitcast.11, bf16[128,128]{1,0:T(8,128)(2,1)} %bitcast.12, bf16[128,128]{1,0:T(8,128)(2,1)} %bitcast.13, bf16[128,2048]{1,0:T(8,128)(2,1)} %args_5_.4, ...), custom_call_target="tpu_custom_call" | custom-call | tf_op jit(solution)/shard_map/mixer/pallas_call | solution.py:729
  60.1 0.8 %copy.12 = bf16[1,128,2048]{2,1,0:T(8,128)(2,1)} copy(bf16[1,128,2048]{2,1,0:T(8,128)(2,1)S(1)} %bitcast.8) | data formatting | bytes 1048576
